TPU v7x, 32 devices: a whole 2x2x4 slice. The times are simulated.
32 devices in a mesh: sp: 8 (over z, x), tp: 4 (over y, core).
Axes of the slice: x: 2, y: 2, z: 4, core: 2. Of those that a mesh axis runs over, the one named last changes fastest.
Arguments:
- queries: bfloat16 [4096, 512], P('sp', 'tp'), may hold values from -9.5625 to 9.5625
- keys: bfloat16 [4096, 512], P('sp', 'tp'), may hold values from -9.5625 to 9.5625
- values: bfloat16 [4096, 512], P('sp', 'tp'), may hold values from -6 to 6
- key_bias: bfloat16 [4096, 8], P('sp', 'tp'), may hold values from -17 to 0
- residual: bfloat16 [4096, 2048], P(('sp', 'tp')), may hold values from -6 to 6
- out_weight: bfloat16 [512, 2048], replicated, may hold values from -1 to 1
- norm_gain: float32 [2048], replicated, may hold values from 0.1 to 1.9
- routes: int32 [4096, 2], P(('sp', 'tp')), may hold values from 0 to 7, all different within a row; in each aligned block of 128 rows (0 to 127, 128 to 255, ...) at most 40 rows name the same one
- route_weights: float32 [4096, 2], P(('sp', 'tp')), may hold values from 0.25 to 2
- gate_weight: bfloat16 [8, 2048, 4096], P('sp', None, 'tp'), may hold values from -0.125 to 0.125
- up_weight: bfloat16 [8, 2048, 4096], P('sp', None, 'tp'), may hold values from -0.125 to 0.125
- down_weight: bfloat16 [8, 4096, 2048], P('sp', 'tp'), may hold values from -0.09375 to 0.09375
Outputs:
- output: bfloat16 [4096, 2048], P(('sp', 'tp'))
Inputs may be any that keep to these rules, and one draw needn't show every extreme that they name: `routes`: each row names 2 different experts; the rows of one device name no expert more than 40 times.
All inputs are finite; a program needn't handle non-finite values.
Results may differ from a plain program's by a relative error of at most 0.017.
Values may be sent and summed in bfloat16 or wider, within the bound.
A program may use at most 128 MiB of HBM per device.

v0:
```python
import jax
import jax.numpy as jnp
from jax import lax
from jax.sharding import PartitionSpec as P

HEAD_DIM = 64
TOP = 2
SPAN = 512
epsilon = 1e-06


def shards(
    queries,
    keys,
    values,
    key_bias,
    residual,
    out_weight,
    norm_gain,
    routes,
    route_weights,
    gate_weight,
    up_weight,
    down_weight,
):
    shard_len = queries.shape[0]
    local_heads = key_bias.shape[1]
    sp_count = lax.axis_size("sp")
    offset = lax.axis_index("sp") * shard_len
    query_heads = queries.reshape(shard_len, local_heads, HEAD_DIM)
    query_pos = offset + lax.iota(jnp.int32, shard_len)
    score_scale = HEAD_DIM ** (-0.5)
    slot_count = sp_count * shard_len // SPAN

    def span_terms(key_rows, value_rows, bias_rows, key_first):
        scores = jnp.einsum(
            "qhd,khd->qhk",
            query_heads,
            key_rows.reshape(SPAN, local_heads, HEAD_DIM),
            preferred_element_type=jnp.float32,
        )
        scores = scores * score_scale + jnp.transpose(bias_rows.astype(jnp.float32))[None, :, :]
        key_pos = key_first + lax.iota(jnp.int32, SPAN)
        earlier = key_pos[None, None, :] < query_pos[:, None, None]
        failure = jnp.where(earlier, jax.nn.log_sigmoid(-scores), 0.0)
        later_sum = lax.cumsum(failure, axis=2, reverse=True) - failure
        weights = jnp.where(earlier, jnp.exp(jax.nn.log_sigmoid(scores) + later_sum), 0.0).astype(
            jnp.bfloat16
        )
        span_out = jnp.einsum(
            "qhk,khd->qhd",
            weights,
            value_rows.reshape(SPAN, local_heads, HEAD_DIM),
            preferred_element_type=jnp.float32,
        )
        return (span_out, jnp.sum(failure, axis=2))

    def skipped():
        return (
            jnp.zeros((shard_len, local_heads, HEAD_DIM), jnp.float32),
            jnp.zeros((shard_len, local_heads), jnp.float32),
        )

    empty_pair = (
        jnp.zeros((slot_count, shard_len, local_heads, HEAD_DIM), jnp.float32),
        jnp.zeros((slot_count, shard_len, local_heads), jnp.float32),
    )
    key_piece = lax.all_gather(keys, "sp", axis=0, tiled=True)
    value_piece = lax.all_gather(values, "sp", axis=0, tiled=True)
    bias_piece = lax.all_gather(key_bias, "sp", axis=0, tiled=True)
    span_total = key_piece.shape[0] // SPAN

    def place_span(which, held):
        outs_held, totals_held = held
        row_begin = which * SPAN

        def compute():
            return span_terms(
                lax.dynamic_slice_in_dim(key_piece, row_begin, SPAN, 0),
                lax.dynamic_slice_in_dim(value_piece, row_begin, SPAN, 0),
                lax.dynamic_slice_in_dim(bias_piece, row_begin, SPAN, 0),
                row_begin,
            )

        span_out, span_sum = lax.cond(row_begin < offset + shard_len, compute, skipped)
        slot = row_begin // SPAN
        return (
            lax.dynamic_update_index_in_dim(outs_held, span_out, slot, 0),
            lax.dynamic_update_index_in_dim(totals_held, span_sum, slot, 0),
        )

    span_outs, span_sums = lax.fori_loop(0, span_total, place_span, empty_pair)
    after_span = lax.cumsum(span_sums, axis=0, reverse=True) - span_sums
    attended = jnp.sum(jnp.exp(after_span)[..., None] * span_outs, axis=0)
    attended = attended.reshape(shard_len, local_heads * HEAD_DIM).astype(jnp.bfloat16)
    token_heads = lax.all_to_all(attended, "tp", split_axis=0, concat_axis=1, tiled=True)
    projected = jnp.dot(token_heads, out_weight, preferred_element_type=jnp.float32)
    stream = (residual.astype(jnp.float32) + projected).astype(jnp.bfloat16).astype(jnp.float32)
    normed = (
        stream * lax.rsqrt(jnp.mean(stream * stream, axis=-1, keepdims=True) + epsilon) * norm_gain
    ).astype(jnp.bfloat16)
    token_count = residual.shape[0]
    width_model = residual.shape[1]
    capacity = max(2, 5 * token_count * TOP // (4 * sp_count))
    flat_routes = routes.reshape(-1)
    onehot = (flat_routes[:, None] == lax.iota(jnp.int32, sp_count)[None, :]).astype(jnp.int32)
    before = jnp.cumsum(onehot, axis=0) - onehot
    slot_of = flat_routes * capacity + jnp.sum(before * onehot, axis=1)
    select = (slot_of[:, None] == lax.iota(jnp.int32, sp_count * capacity)[None, :]).astype(
        jnp.bfloat16
    )
    placing = jnp.sum(select.reshape(token_count, TOP, sp_count * capacity), axis=1)
    outgoing = jnp.einsum("ts,td->sd", placing, normed, preferred_element_type=jnp.float32).astype(
        jnp.bfloat16
    )
    arrived = lax.all_to_all(outgoing, "sp", split_axis=0, concat_axis=0, tiled=True)
    row_block = lax.all_gather(arrived, "tp", axis=0, tiled=True)
    gate_act = jnp.dot(row_block, gate_weight[0], preferred_element_type=jnp.float32)
    up_act = jnp.dot(row_block, up_weight[0], preferred_element_type=jnp.float32)
    hidden = (jax.nn.silu(gate_act) * up_act).astype(jnp.bfloat16)
    partial_value = jnp.dot(hidden, down_weight[0], preferred_element_type=jnp.float32)
    summed = lax.psum_scatter(
        lax.optimization_barrier(partial_value.astype(jnp.bfloat16))
        .astype(jnp.float32)
        .astype(jnp.bfloat16),
        "tp",
        scatter_dimension=0,
        tiled=True,
    )
    returned = lax.all_to_all(summed, "sp", split_axis=0, concat_axis=0, tiled=True)
    picked = jnp.dot(select, returned, preferred_element_type=jnp.float32).reshape(
        token_count, TOP, width_model
    )
    routed = jnp.sum(picked * route_weights[:, :, None], axis=1)
    return (stream + routed).astype(jnp.bfloat16)


def solution(mesh):
    return jax.shard_map(
        shards,
        mesh=mesh,
        in_specs=(
            P("sp", "tp"),
            P("sp", "tp"),
            P("sp", "tp"),
            P("sp", "tp"),
            P(("sp", "tp"), None),
            P(),
            P(),
            P(("sp", "tp"), None),
            P(("sp", "tp"), None),
            P("sp", None, "tp"),
            P("sp", None, "tp"),
            P("sp", "tp", None),
        ),
        out_specs=P(("sp", "tp"), None),
        check_vma=False,
    )
```

profile of v0, /device:TPU:0, one launch (start us, length us, event | category | flops | bytes accessed | tf_op | source)
XLA Modules:
  0.0 488.3 jit_solution(3065898955620560094)
XLA Ops:
  6.5 1.8 copy.63
  8.4 1.7 copy.62
  13.4 28.3 %all_gather.14 = bf16[4096,2]{0,1:T(2,128)(2,1)S(1)} all-gather(bf16[512,2]{0,1:T(2,128)(2,1)} %param.19), channel_id=1, replica_groups=mesh['sp'=8,'tp'=4] {'sp'}, dimensions={0}, use_global_device_ids=true | all-gather | bytes 18432 | tf_op jit(solution)/shard_map/all_gather | solution.py:70
  42.3 9.2 %all-gather.6.cloned.1.call-done = bf16[4096,128]{0,1:T(8,128)(2,1)} async-done(((bf16[512,128]{0,1:T(8,128)(2,1)}), bf16[4096,128]{0,1:T(8,128)(2,1)}) %all-gather.6.cloned.1.call-update) | async-done | bytes 1048592 | tf_op jit(solution)/shard_map/all_gather | solution.py:68
  51.6 40.3 %all-gather.4.cloned.1.call-done = bf16[4096,128]{0,1:T(8,128)(2,1)} async-done(((bf16[512,128]{0,1:T(8,128)(2,1)}), bf16[4096,128]{0,1:T(8,128)(2,1)}) %all-gather.4.cloned.1.call-update) | async-done | bytes 1048592 | tf_op jit(solution)/shard_map/all_gather | solution.py:69
  91.9 1.6 broadcast_in_dim.56
  93.5 28.5 %while.18 = (s32[]{:T(128)}, f32[8,512,2,64]{1,3,2,0:T(8,128)}, f32[8,512,2]{1,2,0:T(2,128)S(1)}, s32[]{:T(128)}, bf16[4096,128]{0,1:T(8,128)(2,1)}, /*index=5*/...) while((s32[]{:T(128)}, f32[8,512,2,64]{1,3,2,0:T(8,128)}, ...), condition=%wide.region_6.7_spmd.clone, body=%wide.region_0.6_spmd.clone.sunk | while | flops 218906624 | bytes 42494496 | solution.py:92
  93.5 22.3 %conditional.3 = (f32[1,512,2,64]{1,3,2,0:T(8,128)S(1)}, f32[1,512,2]{1,2,0:T(2,128)S(1)}) conditional(s32[]{:T(128)} %convert_element_type.94, () %tuple.60, (s32[]{:T(128)}, bf16[4096,128]{0,1:T(8,128)(2,1)}, s32[]{:T(128)}, bf16[4096,128]{0,1:T(8,128)(2,1)}, bf16[512,2,64]{0,2,1:T(8,128)(2,1)S(1)}, /*index=5*/bf16[4096,2]{0,1:T(2,128)(2,1)S(1)}, ...), branch_computations={%region_1.0_spmd, %region_2.5_spmd} | conditional | flops 218906624 | bytes 41959552 | solution.py:85
  94.7 3.0 fusion.15
  97.8 9.6 %fusion.13 = f32[512,2,4,128]{0,2,1,3:T(4,128)S(1)} fusion(f32[512,2,4,128]{0,3,2,1:T(8,128)S(1)} %bitcast.89), kind=kOutput, calls=%fused_computation.18 | output fusion | flops 66584576 | bytes 4194304 | tf_op jit(solution)/shard_map/reduce-window
  107.4 1.3 copy-done.1
  108.8 1.8 broadcast_add_fusion
  110.6 1.2 copy.60
  112.2 3.2 fusion.6
  122.0 1.8 multiply_reduce_fusion
  124.6 3.5 all-to-all-start
  128.2 4.5 all-to-all-done
  132.6 1.6 multiply_reduce_fusion.1
  134.8 190.0 %all_to_all.40 = bf16[8,40,2048]{2,1,0:T(8,128)(2,1)} all-to-all(bf16[8,40,2048]{2,1,0:T(8,128)(2,1)S(1)} %bitcast.92), channel_id=1, replica_groups=mesh['sp'=8,'tp'=4] {'sp'}, dimensions={0} | all-to-all | bytes 2621440 | tf_op jit(solution)/shard_map/all_to_all | solution.py:116
  324.9 38.8 %all-gather.8.cloned.1.call-done = bf16[1280,2048]{1,0:T(8,128)(2,1)} async-done(((bf16[320,2048]{1,0:T(8,128)(2,1)}), bf16[1280,2048]{1,0:T(8,128)(2,1)}) %all-gather.8.cloned.1.call-update) | async-done | bytes 5242896 | tf_op jit(solution)/shard_map/all_gather | solution.py:117
  363.7 10.2 %fusion.18 = f32[1280,1024]{1,0:T(8,128)} fusion(bf16[1280,2048]{1,0:T(8,128)(2,1)} %all-gather.8.cloned.1.call-done, bf16[1,2048,1024]{2,1,0:T(8,128)(2,1)} %param.25), kind=kOutput, calls=%fused_computation.37 | convolution fusion | flops 5368709120 | bytes 14680064 | tf_op jit(solution)/shard_map/dot_general | solution.py:118
  373.9 18.0 %convolution_convert_fusion = bf16[1280,2048]{1,0:T(8,128)(2,1)} fusion(bf16[1,1024,2048]{2,1,0:T(8,128)(2,1)} %param.27, f32[1280,1024]{1,0:T(8,128)} %fusion.18, bf16[1280,2048]{1,0:T(8,128)(2,1)} %all-gather.8.cloned.1.call-done, bf16[1,2048,1024]{2,1,0:T(8,128)(2,1)} %param.26), kind=kOutput, calls=%fused_computation.33 | convolution fusion | flops 10747904000 | bytes 24117248 | tf_op jit(solution)/shard_map/dot_general | solution.py:121
  391.9 51.5 %reduce-scatter.2.cloned.1.call-done = bf16[320,2048]{1,0:T(8,128)(2,1)} async-done(((bf16[1280,2048]{1,0:T(8,128)(2,1)}), bf16[320,2048]{1,0:T(8,128)(2,1)}) %reduce-scatter.2.cloned.1.call-update) | async-done | bytes 1310736 | tf_op jit(solution)/shard_map/reduce_scatter | solution.py:122
  443.4 36.7 %all_to_all.41 = bf16[8,40,2048]{2,1,0:T(8,128)(2,1)S(1)} all-to-all(bf16[8,40,2048]{2,1,0:T(8,128)(2,1)} %bitcast.95), channel_id=1, replica_groups=mesh['sp'=8,'tp'=4] {'sp'}, dimensions={0} | all-to-all | bytes 2621440 | tf_op jit(solution)/shard_map/all_to_all | solution.py:130
  (92 shorter events, 15.4 us)
Async XLA Ops:
  6.5 126.1 %copy-start = (bf16[512,2048]{1,0:T(8,128)(2,1)S(1)}, bf16[512,2048]{1,0:T(8,128)(2,1)}, u32[]{:S(2)}) copy-start(bf16[512,2048]{1,0:T(8,128)(2,1)} %param.21) | copy-start | bytes 6291460
  6.5 45.0 %all-gather.6.cloned.1.call-start = ((), (), s32[]{:S(2)}) async-start(), calls=%async_computation.5 | async-start | bytes 1179648 | tf_op jit(solution)/shard_map/all_gather | solution.py:68
  8.4 83.5 %all-gather.4.cloned.1.call-start = ((), (), s32[]{:S(2)}) async-start(), calls=%async_computation.4 | async-start | bytes 1179648 | tf_op jit(solution)/shard_map/all_gather | solution.py:69
  107.4 1.3 copy-start.1
  110.6 1.6 copy-start.2
  124.6 9.6 %copy-start.3 = (f32[2048]{0:T(1024)S(1)}, f32[2048]{0:T(1024)}, u32[]{:S(2)}) copy-start(f32[2048]{0:T(1024)} %param.22) | copy-start | bytes 24580
  124.6 8.0 %all-to-all-start = ((bf16[4,128,128]{1,2,0:T(8,128)(2,1)}), bf16[4,128,128]{1,2,0:T(8,128)(2,1)S(1)}, u32[]{:S(2)}, u32[]{:S(2)}) async-start(bf16[4,128,128]{1,2,0:T(8,128)(2,1)} %copy.65), calls=%async_computation | async-start | bytes 262144 | tf_op jit(solution)/shard_map/all_to_all | solution.py:96
  128.1 235.7 %all-gather.8.cloned.1.call-start = ((), (), s32[]{:S(2)}) async-start(), calls=%async_computation.6 | async-start | bytes 6553600 | tf_op jit(solution)/shard_map/all_gather | solution.py:117
  324.8 118.6 %reduce-scatter.2.cloned.1.call-start = ((), (), s32[]{:S(2)}) async-start(), calls=%async_computation.7 | async-start | bytes 6553600 | tf_op jit(solution)/shard_map/reduce_scatter | solution.py:122
  391.9 88.2 %copy-start.4 = (f32[128,2]{0,1:T(2,128)S(1)}, f32[128,2]{0,1:T(2,128)}, u32[]{:S(2)}) copy-start(f32[128,2]{0,1:T(2,128)} %param.24) | copy-start | bytes 3076
Sparse Core Ops, SparseCore 0:
  9.4 42.1 all-gather.5
  53.6 38.1 all-gather.3
  325.0 38.7 all-gather.7
  392.0 51.3 reduce-scatter.1
where the time goes:
time: 489 us; the launch traced here: 488 us
  blocking collectives  255 us (52%)
  waiting for transfers between devices  144 us (29%)
  matrix products  34.4 us (7%)
  other arithmetic  19.2 us (4%)
  local copies, waits for them, and re-layouts  18.3 us (4%)
  between operations  13.2 us (3%)
    all_to_all x1, blocking collectives, shards(): lax.all_to_all(outgoing, 'sp', split_axis=0, concat_axis=0, tiled=True)  190 us
    reduce_scatter x1, waiting for transfers between devices, shards(): lax.psum_scatter(lax.optimization_barrier(partial_value.astype(jnp.bfloat...  51.5 us
    all_gather x1, waiting for transfers between devices, shards(): value_piece = lax.all_gather(values, 'sp', axis=0, tiled=True)  40.3 us
    all_gather x1, waiting for transfers between devices, shards(): row_block = lax.all_gather(arrived, 'tp', axis=0, tiled=True)  38.8 us
    all_to_all x1, blocking collectives, shards(): lax.all_to_all(summed, 'sp', split_axis=0, concat_axis=0, tiled=True)  36.7 us
    all_gather x1, blocking collectives, shards(): bias_piece = lax.all_gather(key_bias, 'sp', axis=0, tiled=True)  28.3 us
    dot_general x1, matrix products, shards(): jnp.dot(hidden, down_weight[0], preferred_element_type=jnp.float32)  18 us
    another operation x4, other arithmetic  10.3 us
  transfers between devices with their start and end apart: 5, of which 5 were waited for; matrix products, arithmetic and copies ran while one was open for 1% of the time, Pallas kernels for 0%

commit v1 on v0

--- a/solution.py
+++ b/solution.py
@@ -66,7 +66,12 @@
         jnp.zeros((slot_count, shard_len, local_heads), jnp.float32),
     )
     key_piece = lax.all_gather(keys, "sp", axis=0, tiled=True)
-    value_piece = lax.all_gather(values, "sp", axis=0, tiled=True)
+    ring = [values]
+    for hop in range(7):
+        ring.append(lax.ppermute(ring[-1], "sp", [(dev, (dev + 1) % 8) for dev in range(8)]))
+    value_piece = jnp.roll(
+        jnp.concatenate(ring[::-1], axis=0), (lax.axis_index("sp") + 1) * ring[0].shape[0], axis=0
+    )
     bias_piece = lax.all_gather(key_bias, "sp", axis=0, tiled=True)
     span_total = key_piece.shape[0] // SPAN
 

time: 489 us -> 517 us (1.057)
  blocking collectives: 255 us -> 277 us
  waiting for transfers between devices: 144 us -> 133 us
  local copies, waits for them, and re-layouts: 18.3 us -> 24.5 us
    all_gather x1 -> x0, waiting for transfers between devices: 40.3 us -> none  [shards(): value_piece = lax.all_gather(values, 'sp', axis=0, tiled=True)]
    ppermute x0 -> x7, waiting for transfers between devices: none -> 38.4 us  [shards(): lax.ppermute(ring[-1], 'sp', [(dev, (dev + 1) % 8) for dev in range(8)])]
    all_to_all x1, blocking collectives: 190 us -> 213 us  [shards(): lax.all_to_all(outgoing, 'sp', split_axis=0, concat_axis=0, tiled=True)]
    all_gather x1, waiting for transfers between devices: 9.23 us -> 0.02 us  [shards(): key_piece = lax.all_gather(keys, 'sp', axis=0, tiled=True)]
  transfers between devices with their start and end apart: 5 -> 11, of which waited for: 5 -> 9; matrix products, arithmetic and copies ran while one was open for 1% -> 1% of each run, Pallas kernels for 0% -> 0%
where the time goes in v1:
time: 517 us; the launch traced here: 515 us
  blocking collectives  277 us (54%)
  waiting for transfers between devices  133 us (26%)
  matrix products  36 us (7%)
  local copies, waits for them, and re-layouts  24.5 us (5%)
  other arithmetic  21.9 us (4%)
  between operations  13.4 us (3%)
  starting transfers between devices  8.68 us (2%)
    all_to_all x1, blocking collectives, shards(): lax.all_to_all(outgoing, 'sp', split_axis=0, concat_axis=0, tiled=True)  213 us
    reduce_scatter x1, waiting for transfers between devices, shards(): lax.psum_scatter(lax.optimization_barrier(partial_value.astype(jnp.bfloat...  51.5 us
    all_gather x1, waiting for transfers between devices, shards(): row_block = lax.all_gather(arrived, 'tp', axis=0, tiled=True)  38.8 us
    ppermute x7, waiting for transfers between devices, shards(): lax.ppermute(ring[-1], 'sp', [(dev, (dev + 1) % 8) for dev in range(8)])  38.4 us
    all_to_all x1, blocking collectives, shards(): lax.all_to_all(summed, 'sp', split_axis=0, concat_axis=0, tiled=True)  36.7 us
    all_gather x1, blocking collectives, shards(): bias_piece = lax.all_gather(key_bias, 'sp', axis=0, tiled=True)  27.4 us
    dot_general x1, matrix products, shards(): jnp.dot(hidden, down_weight[0], preferred_element_type=jnp.float32)  18 us
    another operation x4, other arithmetic  10.9 us
  transfers between devices with their start and end apart: 11, of which 9 were waited for; matrix products, arithmetic and copies ran while one was open for 1% of the time, Pallas kernels for 0%

profile of v1, /device:TPU:0, one launch (start us, length us, event | category | flops | bytes accessed | tf_op | source)
XLA Modules:
  0.0 514.7 jit_solution(582905120616945762)
XLA Ops:
  7.7 3.0 collective-permute-start
  10.7 6.5 %collective-permute-done = bf16[512,128]{0,1:T(8,128)(2,1)S(1)} collective-permute-done((bf16[512,128]{0,1:T(8,128)(2,1)S(1)}, bf16[512,128]{0,1:T(8,128)(2,1)S(1)}, u32[]{:S(2)}, u32[]{:S(2)}) %collective-permute-start) | collective-permute-done | bytes 131104 | tf_op jit(solution)/shard_map/ppermute | solution.py:71
  17.3 7.7 %collective-permute-done.1 = bf16[512,128]{0,1:T(8,128)(2,1)S(1)} collective-permute-done((bf16[512,128]{0,1:T(8,128)(2,1)S(1)}, bf16[512,128]{0,1:T(8,128)(2,1)S(1)}, u32[]{:S(2)}, u32[]{:S(2)}) %collective-permute-start.1) | collective-permute-done | bytes 131104 | tf_op jit(solution)/shard_map/ppermute | solution.py:71
  24.9 7.7 %collective-permute-done.2 = bf16[512,128]{0,1:T(8,128)(2,1)S(1)} collective-permute-done((bf16[512,128]{0,1:T(8,128)(2,1)S(1)}, bf16[512,128]{0,1:T(8,128)(2,1)S(1)}, u32[]{:S(2)}, u32[]{:S(2)}) %collective-permute-start.2) | collective-permute-done | bytes 131104 | tf_op jit(solution)/shard_map/ppermute | solution.py:71
  35.2 5.0 collective-permute-done.3
  40.8 7.2 %collective-permute-done.4 = bf16[512,128]{0,1:T(8,128)(2,1)S(1)} collective-permute-done((bf16[512,128]{0,1:T(8,128)(2,1)S(1)}, bf16[512,128]{0,1:T(8,128)(2,1)S(1)}, u32[]{:S(2)}, u32[]{:S(2)}) %collective-permute-start.4) | collective-permute-done | bytes 131104 | tf_op jit(solution)/shard_map/ppermute | solution.py:71
  50.5 27.4 %all_gather.10 = bf16[4096,2]{0,1:T(2,128)(2,1)} all-gather(bf16[512,2]{0,1:T(2,128)(2,1)} %param.19), channel_id=1, replica_groups=mesh['sp'=8,'tp'=4] {'sp'}, dimensions={0}, use_global_device_ids=true | all-gather | bytes 18432 | tf_op jit(solution)/shard_map/all_gather | solution.py:75
  77.8 2.1 collective-permute-start.6
  81.2 4.3 collective-permute-done.6
  88.1 36.7 %while.18 = (s32[]{:T(128)}, f32[8,512,2,64]{1,3,2,0:T(8,128)}, f32[8,512,2]{1,2,0:T(2,128)}, s32[]{:T(128)}, bf16[4096,128]{0,1:T(8,128)(2,1)S(1)}, /*index=5*/...) while((s32[]{:T(128)}, f32[8,512,2,64]{1,3,2,0:T(8,128)}, ...), condition=%wide.region_6.7_spmd.clone, body=%wide.region_0.6_spmd.clone.sunk | while | flops 218906624 | bytes 42543728 | solution.py:97
  88.1 25.8 %conditional.3 = (f32[1,512,2,64]{1,3,2,0:T(8,128)S(1)}, f32[1,512,2]{1,2,0:T(2,128)S(1)}) conditional(s32[]{:T(128)} %convert_element_type.94, () %tuple.60, (s32[]{:T(128)}, bf16[4096,128]{0,1:T(8,128)(2,1)S(1)}, s32[]{:T(128)}, bf16[4096,128]{0,1:T(8,128)(2,1)}, bf16[512,2,64]{0,2,1:T(8,128)(2,1)}, /*index=5*/bf16[4096,2]{0,1:T(2,128)(2,1)}, ...), branch_computations={%region_1.1_spmd, %region_2.5_spmd} | conditional | flops 218906624 | bytes 42008788 | solution.py:90
  90.0 4.6 fusion.15
  94.6 9.6 %fusion.13 = f32[512,2,4,128]{0,2,1,3:T(4,128)S(1)} fusion(f32[512,2,4,128]{0,3,2,1:T(8,128)S(1)} %bitcast.89), kind=kOutput, calls=%fused_computation.18 | output fusion | flops 66584576 | bytes 4194304 | tf_op jit(solution)/shard_map/reduce-window
  106.9 1.8 broadcast_add_fusion
  110.4 3.2 fusion.6
  125.7 1.9 multiply_reduce_fusion
  128.2 3.5 all-to-all-start
  131.8 4.5 all-to-all-done
  138.5 212.7 %all_to_all.40 = bf16[8,40,2048]{2,1,0:T(8,128)(2,1)} all-to-all(bf16[8,40,2048]{2,1,0:T(8,128)(2,1)S(1)} %bitcast.92), channel_id=1, replica_groups=mesh['sp'=8,'tp'=4] {'sp'}, dimensions={0} | all-to-all | bytes 2621440 | tf_op jit(solution)/shard_map/all_to_all | solution.py:121
  351.2 38.8 %all-gather.5.cloned.1.call-done = bf16[1280,2048]{1,0:T(8,128)(2,1)} async-done(((bf16[320,2048]{1,0:T(8,128)(2,1)}), bf16[1280,2048]{1,0:T(8,128)(2,1)}) %all-gather.5.cloned.1.call-update) | async-done | bytes 5242896 | tf_op jit(solution)/shard_map/all_gather | solution.py:122
  390.1 10.2 %fusion.18 = f32[1280,1024]{1,0:T(8,128)} fusion(bf16[1280,2048]{1,0:T(8,128)(2,1)} %all-gather.5.cloned.1.call-done, bf16[1,2048,1024]{2,1,0:T(8,128)(2,1)} %param.25), kind=kOutput, calls=%fused_computation.37 | convolution fusion | flops 5368709120 | bytes 14680064 | tf_op jit(solution)/shard_map/dot_general | solution.py:123
  400.3 18.0 %convolution_convert_fusion = bf16[1280,2048]{1,0:T(8,128)(2,1)} fusion(bf16[1,1024,2048]{2,1,0:T(8,128)(2,1)} %param.27, f32[1280,1024]{1,0:T(8,128)} %fusion.18, bf16[1280,2048]{1,0:T(8,128)(2,1)} %all-gather.5.cloned.1.call-done, bf16[1,2048,1024]{2,1,0:T(8,128)(2,1)} %param.26), kind=kOutput, calls=%fused_computation.33 | convolution fusion | flops 10747904000 | bytes 24117248 | tf_op jit(solution)/shard_map/dot_general | solution.py:126
  418.2 51.5 %reduce-scatter.2.cloned.1.call-done = bf16[320,2048]{1,0:T(8,128)(2,1)} async-done(((bf16[1280,2048]{1,0:T(8,128)(2,1)}), bf16[320,2048]{1,0:T(8,128)(2,1)}) %reduce-scatter.2.cloned.1.call-update) | async-done | bytes 1310736 | tf_op jit(solution)/shard_map/reduce_scatter | solution.py:127
  469.7 36.7 %all_to_all.41 = bf16[8,40,2048]{2,1,0:T(8,128)(2,1)S(1)} all-to-all(bf16[8,40,2048]{2,1,0:T(8,128)(2,1)} %bitcast.95), channel_id=1, replica_groups=mesh['sp'=8,'tp'=4] {'sp'}, dimensions={0} | all-to-all | bytes 2621440 | tf_op jit(solution)/shard_map/all_to_all | solution.py:135
  (128 shorter events, 33.4 us)
Async XLA Ops:
  6.5 129.7 %copy-start = (bf16[512,2048]{1,0:T(8,128)(2,1)S(1)}, bf16[512,2048]{1,0:T(8,128)(2,1)}, u32[]{:S(2)}) copy-start(bf16[512,2048]{1,0:T(8,128)(2,1)} %param.21) | copy-start | bytes 6291460
  6.5 79.4 %all-gather.3.cloned.1.call-start = ((), (), s32[]{:S(2)}) async-start(), calls=%async_computation.4 | async-start | bytes 1179648 | tf_op jit(solution)/shard_map/all_gather | solution.py:68
  7.7 9.6 %collective-permute-start = (bf16[512,128]{0,1:T(8,128)(2,1)S(1)}, bf16[512,128]{0,1:T(8,128)(2,1)S(1)}, u32[]{:S(2)}, u32[]{:S(2)}) collective-permute-start(bf16[512,128]{0,1:T(8,128)(2,1)S(1)} %copy.70), channel_id=1, source_target_pairs={{0,4},{4,8},{8,12},{12,16},{16,20},{20,24},{24,28},{28,0},{1,5},{5... | collective-permute-start | bytes 393224 | tf_op jit(solution)/shard_map/ppermute | solution.py:71
  17.3 7.7 %collective-permute-start.1 = (bf16[512,128]{0,1:T(8,128)(2,1)S(1)}, bf16[512,128]{0,1:T(8,128)(2,1)S(1)}, u32[]{:S(2)}, u32[]{:S(2)}) collective-permute-start(bf16[512,128]{0,1:T(8,128)(2,1)S(1)} %collective-permute-done), channel_id=1, source_target_pairs={{0,4},{4,8},{8,12},{12,16},{16,20},{20,24},{24,28},{28,0},{1,5},{5... | collective-permute-start | bytes 393224 | tf_op jit(solution)/shard_map/ppermute | solution.py:71
  24.9 7.7 %collective-permute-start.2 = (bf16[512,128]{0,1:T(8,128)(2,1)S(1)}, bf16[512,128]{0,1:T(8,128)(2,1)S(1)}, u32[]{:S(2)}, u32[]{:S(2)}) collective-permute-start(bf16[512,128]{0,1:T(8,128)(2,1)S(1)} %collective-permute-done.1), channel_id=1, source_target_pairs={{0,4},{4,8},{8,12},{12,16},{16,20},{20,24},{24,28},{28,0},{1,5},{5... | collective-permute-start | bytes 393224 | tf_op jit(solution)/shard_map/ppermute | solution.py:71
  32.6 7.7 %collective-permute-start.3 = (bf16[512,128]{0,1:T(8,128)(2,1)S(1)}, bf16[512,128]{0,1:T(8,128)(2,1)S(1)}, u32[]{:S(2)}, u32[]{:S(2)}) collective-permute-start(bf16[512,128]{0,1:T(8,128)(2,1)S(1)} %collective-permute-done.2), channel_id=1, source_target_pairs={{0,4},{4,8},{8,12},{12,16},{16,20},{20,24},{24,28},{28,0},{1,5},{5... | collective-permute-start | bytes 393224 | tf_op jit(solution)/shard_map/ppermute | solution.py:71
  40.3 7.8 %collective-permute-start.4 = (bf16[512,128]{0,1:T(8,128)(2,1)S(1)}, bf16[512,128]{0,1:T(8,128)(2,1)S(1)}, u32[]{:S(2)}, u32[]{:S(2)}) collective-permute-start(bf16[512,128]{0,1:T(8,128)(2,1)S(1)} %collective-permute-done.3), channel_id=1, source_target_pairs={{0,4},{4,8},{8,12},{12,16},{16,20},{20,24},{24,28},{28,0},{1,5},{5... | collective-permute-start | bytes 393224 | tf_op jit(solution)/shard_map/ppermute | solution.py:71
  48.1 29.8 %collective-permute-start.5 = (bf16[512,128]{0,1:T(8,128)(2,1)S(1)}, bf16[512,128]{0,1:T(8,128)(2,1)S(1)}, u32[]{:S(2)}, u32[]{:S(2)}) collective-permute-start(bf16[512,128]{0,1:T(8,128)(2,1)S(1)} %collective-permute-done.4), channel_id=1, source_target_pairs={{0,4},{4,8},{8,12},{12,16},{16,20},{20,24},{24,28},{28,0},{1,5},{5... | collective-permute-start | bytes 393224 | tf_op jit(solution)/shard_map/ppermute | solution.py:71
  77.8 7.7 %collective-permute-start.6 = (bf16[512,128]{0,1:T(8,128)(2,1)S(1)}, bf16[512,128]{0,1:T(8,128)(2,1)S(1)}, u32[]{:S(2)}, u32[]{:S(2)}) collective-permute-start(bf16[512,128]{0,1:T(8,128)(2,1)S(1)} %collective-permute-done.5), channel_id=1, source_target_pairs={{0,4},{4,8},{8,12},{12,16},{16,20},{20,24},{24,28},{28,0},{1,5},{5... | collective-permute-start | bytes 393224 | tf_op jit(solution)/shard_map/ppermute | solution.py:71
  89.7 4.8 copy-start.3
  104.2 1.3 copy-start.1
  108.8 1.6 copy-start.2
  108.8 1.6 copy-start.4
  110.4 3.5 copy-start.5
  124.8 7.0 %copy-start.7 = (s32[128,2]{0,1:T(2,128)S(1)}, s32[128,2]{0,1:T(2,128)}, u32[]{:S(2)}) copy-start(s32[128,2]{0,1:T(2,128)} %multiply_add_fusion.1) | copy-start | bytes 3076
  128.2 9.6 %copy-start.6 = (f32[2048]{0:T(1024)S(1)}, f32[2048]{0:T(1024)}, u32[]{:S(2)}) copy-start(f32[2048]{0:T(1024)} %param.22) | copy-start | bytes 24580
  128.2 8.0 %all-to-all-start = ((bf16[4,128,128]{1,2,0:T(8,128)(2,1)}), bf16[4,128,128]{1,2,0:T(8,128)(2,1)S(1)}, u32[]{:S(2)}, u32[]{:S(2)}) async-start(bf16[4,128,128]{1,2,0:T(8,128)(2,1)} %copy.75), calls=%async_computation | async-start | bytes 262144 | tf_op jit(solution)/shard_map/all_to_all | solution.py:101
  131.7 258.3 %all-gather.5.cloned.1.call-start = ((), (), s32[]{:S(2)}) async-start(), calls=%async_computation.5 | async-start | bytes 6553600 | tf_op jit(solution)/shard_map/all_gather | solution.py:122
  351.2 118.6 %reduce-scatter.2.cloned.1.call-start = ((), (), s32[]{:S(2)}) async-start(), calls=%async_computation.6 | async-start | bytes 6553600 | tf_op jit(solution)/shard_map/reduce_scatter | solution.py:127
  418.2 88.2 %copy-start.8 = (f32[128,2]{0,1:T(2,128)S(1)}, f32[128,2]{0,1:T(2,128)}, u32[]{:S(2)}) copy-start(f32[128,2]{0,1:T(2,128)} %param.24) | copy-start | bytes 3076
Sparse Core Ops, SparseCore 0:
  34.4 42.6 all-gather.2
  351.3 38.7 all-gather.4
  418.4 51.3 reduce-scatter.1
